TPU v7x, 512 devices: a whole 4x4x16 slice. The times are simulated.
512 devices in a mesh: kv: 16 (over y, x), tp: 32 (over z, core).
Axes of the slice: x: 4, y: 4, z: 16, core: 2. Of those that a mesh axis runs over, the one named last changes fastest.
Arguments:
- residual: bfloat16 [512, 2048], P('tp', 'kv'), may hold values from -64 to 64
- prior_state: float32 [512, 16, 128, 128], P('tp', 'kv'), may hold values from -6 to 6
- w_query: bfloat16 [2048, 2048], P('tp', 'kv'), may hold values from -0.125 to 0.125
- w_forget: bfloat16 [2048, 2048], P('tp', 'kv'), may hold values from -0.125 to 0.125
- w_value: bfloat16 [2048, 2048], P('tp', 'kv'), may hold values from -0.125 to 0.125
- w_outgate: bfloat16 [2048, 2048], P('tp', 'kv'), may hold values from -0.125 to 0.125
- forget_floor: float32 [2048], P('kv'), may hold values from 0.05 to 0.9
- group_gain: float32 [2048], P('kv'), may hold values from 0.1 to 1.9
- w_mix_out: bfloat16 [2048, 2048], P('kv', 'tp'), may hold values from -0.397747564 to 0.397747564
- gain_mix_pre: float32 [2048], replicated, may hold values from 0.1 to 1.9
- gain_mix_post: float32 [2048], replicated, may hold values from 0.05 to 1.9
- gain_mlp_pre: float32 [2048], replicated, may hold values from 0.1 to 1.9
- gain_mlp_post: float32 [2048], replicated, may hold values from 0.1 to 1.9
- w_up: bfloat16 [2048, 8192], P('tp', 'kv'), may hold values from -0.125 to 0.125
- w_down: bfloat16 [8192, 2048], P('kv', 'tp'), may hold values from -0.198873782 to 0.198873782
Outputs:
- layer_out: bfloat16 [512, 2048], P('tp', 'kv')
- new_state: float32 [512, 16, 128, 128], P('tp', 'kv')
All inputs are finite; a program needn't handle non-finite values.
Results may differ from a plain program's by a relative error of at most 0.015.
Values may be sent and summed in bfloat16 or wider, within the bound.
No kernel may reach another device: no remote copies, remote signals or barrier semaphores. Data moves between devices by JAX's collectives and lax.ppermute only.
A program may use at most 64 MiB of HBM per device.

v0:
```python
import jax
import jax.numpy as jnp
from jax import lax
from jax.sharding import PartitionSpec as P

HEAD_DIM = 128
epsilon = 1e-06


def side_by_side(arrays, axis, dim, along):
    widths = [a.shape[along] for a in arrays]
    both = jnp.concatenate(arrays, axis=along)
    filled = lax.all_gather(both, axis, axis=dim, tiled=True)
    return tuple(jnp.split(filled, [sum(widths[:k]) for k in range(1, len(widths))], axis=along))


def split_up(value, dim, devices):
    before, after = (value.shape[:dim], value.shape[dim + 1 :])
    return jnp.moveaxis(value.reshape(*before, devices, -1, *after), dim, 0)


def summed_on_arrival(value, axis, dim):
    devices = lax.axis_size(axis)
    blocks = lax.all_to_all(split_up(value, dim, devices), axis, 0, 0, tiled=True)
    return jnp.sum(blocks, axis=0)


def from_everyone(value, axis):
    devices = lax.axis_size(axis)
    return lax.all_to_all(
        jnp.broadcast_to(value[None], (devices, *value.shape)), axis, 0, 0, tiled=True
    )


def taken_together(value, axis):
    return from_everyone(value, axis).sum(axis=0)


def inverse_norm(values):
    return lax.rsqrt(jnp.mean(values * values, axis=-1, keepdims=True) + epsilon)


def shards(
    residual,
    prior_state,
    w_query,
    w_forget,
    w_value,
    w_outgate,
    forget_floor,
    group_gain,
    w_mix_out,
    gain_mix_pre,
    gain_mix_post,
    gain_mlp_pre,
    gain_mlp_post,
    w_up,
    w_down,
):
    batch_rows = residual.shape[0]
    own_cols = residual.shape[1]
    offset = lax.axis_index("kv") * own_cols
    whole_rows = lax.all_gather(residual, "kv", axis=1, tiled=True)
    full_width = whole_rows.shape[1]
    stream = whole_rows.astype(jnp.float32)
    normed = (stream * inverse_norm(stream) * gain_mix_pre).astype(jnp.bfloat16)
    pieces = side_by_side((w_query, w_forget, w_value, w_outgate), "tp", 0, 1)
    left_part = normed
    totals = tuple(
        (
            jnp.dot(left_part, weight_part, preferred_element_type=jnp.float32)
            for weight_part in pieces
        )
    )
    query_pre, forget_pre, value_pre, gate_pre = (
        running.astype(jnp.bfloat16) for running in totals
    )
    heads_here = prior_state.shape[1]
    head_shape = (batch_rows, heads_here, HEAD_DIM)
    query_act = jax.nn.silu(query_pre.astype(jnp.float32)).reshape(head_shape)
    lower_bound = forget_floor.reshape(heads_here, HEAD_DIM)
    forget = lower_bound + (1.0 - lower_bound) * jax.nn.sigmoid(
        forget_pre.astype(jnp.float32).reshape(head_shape)
    )
    values_in = value_pre.astype(jnp.float32).reshape(head_shape)
    new_state = (
        forget[..., None] * prior_state + (1.0 - forget)[..., None] * values_in[:, :, None, :]
    )
    readout = jnp.einsum("bhk,bhkv->bhv", query_act, new_state, precision=lax.Precision.HIGHEST)
    gate_act = jax.nn.sigmoid(gate_pre.astype(jnp.float32).reshape(head_shape))
    gated_out = (
        readout * inverse_norm(readout) * group_gain.reshape(heads_here, HEAD_DIM) * gate_act
    ).astype(jnp.bfloat16)
    gated_flat = gated_out.reshape(batch_rows, heads_here * HEAD_DIM)
    mixed_part = jnp.dot(
        gated_flat,
        lax.all_gather(w_mix_out, "tp", axis=1, tiled=True),
        preferred_element_type=jnp.float32,
    )
    mixed_sum = summed_on_arrival(mixed_part, "kv", 1)
    mix_total = taken_together(jnp.sum(mixed_sum * mixed_sum, axis=1), "kv")
    mix_scale = lax.rsqrt(mix_total / full_width + epsilon)[:, None]
    post_gain = lax.dynamic_slice_in_dim(gain_mix_post, offset, own_cols, 0)
    after_mix = (residual.astype(jnp.float32) + mixed_sum * mix_scale * post_gain).astype(
        jnp.bfloat16
    )
    after_wide = after_mix.astype(jnp.float32)
    stream_total = lax.psum(jnp.sum(after_wide * after_wide, axis=1), "kv")
    stream_scale = lax.rsqrt(stream_total / full_width + epsilon)[:, None]
    pre_gain = lax.dynamic_slice_in_dim(gain_mlp_pre, offset, own_cols, 0)
    hidden_own = (after_wide * stream_scale * pre_gain).astype(jnp.bfloat16)
    hidden_in = lax.all_gather(hidden_own, "kv", axis=1, tiled=True)
    left_part = hidden_in
    up_sum = jnp.dot(
        left_part,
        lax.all_gather(w_up, "tp", axis=0, tiled=True),
        preferred_element_type=jnp.float32,
    )
    squared = jnp.square(jax.nn.relu(up_sum)).astype(jnp.bfloat16)
    channel_part = jnp.dot(
        squared,
        lax.all_gather(w_down, "tp", axis=1, tiled=True),
        preferred_element_type=jnp.float32,
    )
    out_gain = lax.dynamic_slice_in_dim(gain_mlp_post, offset, own_cols, 0)
    own_part = summed_on_arrival(channel_part, "kv", 1)
    layer_out = (after_mix.astype(jnp.float32) + own_part * out_gain).astype(jnp.bfloat16)
    return (layer_out, new_state)


def solution(mesh):
    return jax.shard_map(
        shards,
        mesh=mesh,
        in_specs=(
            P("tp", "kv"),
            P("tp", "kv", None, None),
            P("tp", "kv"),
            P("tp", "kv"),
            P("tp", "kv"),
            P("tp", "kv"),
            P("kv"),
            P("kv"),
            P("kv", "tp"),
            P(),
            P(),
            P(),
            P(),
            P("tp", "kv"),
            P("kv", "tp"),
        ),
        out_specs=(P("tp", "kv"), P("tp", "kv", None, None)),
        check_vma=False,
    )
```

profile of v0, /device:TPU:1, one launch (start us, length us, event | category | flops | bytes accessed | tf_op | source)
XLA Modules:
  0.0 254.0 jit_solution(2061126913411901489)
XLA Ops:
  7.2 1.5 pad_maximum_fusion
  8.8 0.7 all-gather.6.cloned.1.call-update
  9.6 0.7 all-gather.8.cloned.1.call-update
  10.2 19.4 %all_gather.18 = bf16[16,2048]{1,0:T(8,128)(2,1)S(1)} all-gather(bf16[16,128]{1,0:T(8,128)(2,1)} %param.15), channel_id=1, replica_groups=mesh['kv'=16,'tp'=32] {'kv'}, dimensions={1}, use_global_device_ids=true | all-gather | bytes 69632 | tf_op jit(solution)/shard_map/all_gather | solution.py:63
  29.7 0.1 fusion.26
  29.8 0.7 broadcast_subtract_fusion.1
  30.5 44.0 %all_gather.20 = bf16[128,2048]{0,1:T(8,128)(2,1)S(1)} all-gather(bf16[128,64]{0,1:T(8,128)(2,1)} %param.23), channel_id=1, replica_groups=mesh['kv'=16,'tp'=32] {'tp'}, dimensions={1}, use_global_device_ids=true | all-gather | bytes 540672 | tf_op jit(solution)/shard_map/all_gather | solution.py:97
  74.5 13.5 %all-gather.4.cloned.1.call-done = bf16[2048,512]{1,0:T(8,128)(2,1)} async-done(((bf16[64,512]{1,0:T(8,128)(2,1)}), bf16[2048,512]{1,0:T(8,128)(2,1)}) %all-gather.4.cloned.1.call-update) | async-done | bytes 2097168 | tf_op jit(solution)/shard_map/all_gather | solution.py:13
  87.9 1.3 fusion.9
  89.2 1.3 divide_multiply_fusion
  90.6 1.3 broadcast_subtract_fusion
  91.9 0.6 multiply_add_fusion
  92.5 1.0 fusion.19
  93.5 0.1 multiply_reduce_fusion.1
  93.6 1.5 convolution_bitcast_fusion
  95.1 13.2 %all_to_all.16 = f32[16,16,128]{2,1,0:T(8,128)S(1)} all-to-all(f32[16,16,128]{2,1,0:T(8,128)S(1)} %convolution_bitcast_fusion), channel_id=1, replica_groups=mesh['kv'=16,'tp'=32] {'kv'}, dimensions={0} | all-to-all | bytes 262144 | tf_op jit(solution)/shard_map/all_to_all | solution.py:24
  108.4 0.1 multiply_reduce_fusion
  108.5 0.6 broadcast_in_dim.2
  109.1 3.4 %all-to-all-start.1 = ((f32[16,1,16]{2,1,0:T(1,128)}), f32[16,1,16]{2,1,0:T(1,128)S(1)}, u32[]{:S(2)}, u32[]{:S(2)}) async-start(f32[16,1,16]{2,1,0:T(1,128)} %broadcast_in_dim.2), calls=%async_computation.1 | async-start | bytes 16384 | tf_op jit(solution)/shard_map/all_to_all | solution.py:30
  112.6 0.8 dynamic_slice.9
  113.3 0.8 dynamic_slice.10
  114.1 4.7 %all-to-all-done.1 = f32[16,1,16]{2,1,0:T(1,128)S(1)} async-done(((f32[16,1,16]{2,1,0:T(1,128)}), f32[16,1,16]{2,1,0:T(1,128)S(1)}, u32[]{:S(2)}, u32[]{:S(2)}) %all-to-all-start.1) | async-done | bytes 1056 | tf_op jit(solution)/shard_map/all_to_all | solution.py:30
  118.8 0.2 fusion.30
  119.0 30.4 %psum.7 = f32[16]{0:T(128)S(1)} all-reduce(f32[16]{0:T(128)S(1)} %get-tuple-element.2), channel_id=1, replica_groups=mesh['kv'=16,'tp'=32] {'kv'}, use_global_device_ids=true, to_apply=%region_6.7 | all-reduce | flops 16 | bytes 128 | tf_op jit(solution)/shard_map/psum | solution.py:108
  149.5 16.5 %all_gather.21 = bf16[16,2048]{1,0:T(8,128)(2,1)S(1)} all-gather(bf16[16,128]{1,0:T(8,128)(2,1)S(1)} %fusion.32), channel_id=1, replica_groups=mesh['kv'=16,'tp'=32] {'kv'}, dimensions={1}, use_global_device_ids=true | all-gather | bytes 69632 | tf_op jit(solution)/shard_map/all_gather | solution.py:112
  166.0 63.7 %all-gather.8.cloned.1.call-done = bf16[512,2048]{0,1:T(8,128)(2,1)} async-done(((bf16[512,64]{0,1:T(8,128)(2,1)}), bf16[512,2048]{0,1:T(8,128)(2,1)}) %all-gather.8.cloned.1.call-update) | async-done | bytes 2097168 | tf_op jit(solution)/shard_map/all_gather | solution.py:122
  229.7 3.2 %convolution_bitcast_fusion.1 = f32[2,16,8,128]{3,2,1,0:T(8,128)S(1)} fusion(bf16[512,2048]{0,1:T(8,128)(2,1)} %all-gather.8.cloned.1.call-done, bf16[16,2048]{1,0:T(8,128)(2,1)S(1)} %all_gather.21, bf16[2048,512]{1,0:T(8,128)(2,1)} %all-gather.6.cloned.1.call-done), kind=kOutput, calls=%fused_computation.1 | convolution fusion | flops 67133440 | bytes 4390912 | tf_op jit(solution)/shard_map/dot_general | solution.py:120
  232.9 0.7 copy.25
  233.5 6.5 %all-to-all-start.2 = ((f32[16,16,128]{2,1,0:T(8,128)}), f32[16,16,128]{2,1,0:T(8,128)S(1)}, u32[]{:S(2)}, u32[]{:S(2)}) async-start(f32[16,16,128]{2,1,0:T(8,128)} %bitcast.30), calls=%async_computation.2 | async-start | bytes 262144 | tf_op jit(solution)/shard_map/all_to_all | solution.py:24
  240.1 0.8 dynamic_slice.11
  240.8 6.1 %all-to-all-done.2 = f32[16,16,128]{2,1,0:T(8,128)S(1)} async-done(((f32[16,16,128]{2,1,0:T(8,128)}), f32[16,16,128]{2,1,0:T(8,128)S(1)}, u32[]{:S(2)}, u32[]{:S(2)}) %all-to-all-start.2) | async-done | bytes 131104 | tf_op jit(solution)/shard_map/all_to_all | solution.py:24
  246.9 0.6 fusion.33
  (25 shorter events, 0.4 us)
Async XLA Ops:
  7.2 83.4 %copy-start.5 = (f32[128]{0:T(128)S(1)}, f32[128]{0:T(128)}, u32[]{:S(2)}) copy-start(f32[128]{0:T(128)} %param.21) | copy-start | bytes 1540
  7.2 83.4 %copy-start.3 = (f32[2048]{0:T(1024)S(1)}, f32[2048]{0:T(1024)}, u32[]{:S(2)}) copy-start(f32[2048]{0:T(1024)} %param.24) | copy-start | bytes 24580
  7.2 84.7 %copy-start.1 = (f32[16,1,128,128]{3,2,1,0:T(8,128)S(1)}, f32[16,1,128,128]{3,2,1,0:T(8,128)}, u32[]{:S(2)}) copy-start(f32[16,1,128,128]{3,2,1,0:T(8,128)} %param.16) | copy-start | bytes 3145732
  7.2 80.7 %all-gather.4.cloned.1.call-start = ((), (), s32[]{:S(2)}) async-start(), calls=%async_computation.3 | async-start | bytes 2162688 | tf_op jit(solution)/shard_map/all_gather | solution.py:13
  8.8 157.2 %all-gather.6.cloned.1.call-start = ((), (), s32[]{:S(2)}) async-start(), calls=%async_computation.4 | async-start | bytes 2162688 | tf_op jit(solution)/shard_map/all_gather | solution.py:116
  9.5 220.2 %all-gather.8.cloned.1.call-start = ((), (), s32[]{:S(2)}) async-start(), calls=%async_computation.5 | async-start | bytes 2162688 | tf_op jit(solution)/shard_map/all_gather | solution.py:122
  90.6 3.1 %copy-start.4 = (f32[128]{0:T(128)S(1)}, f32[128]{0:T(128)}, u32[]{:S(2)}) copy-start(f32[128]{0:T(128)} %param.22) | copy-start | bytes 1540
  91.9 26.9 %copy-start.2 = (bf16[16,128]{1,0:T(8,128)(2,1)S(1)}, bf16[16,128]{1,0:T(8,128)(2,1)}, u32[]{:S(2)}) copy-start(bf16[16,128]{1,0:T(8,128)(2,1)} %param.15) | copy-start | bytes 12292
  92.5 140.3 %copy-start = (f32[16,1,128,128]{3,2,1,0:T(8,128)}, f32[16,1,128,128]{3,2,1,0:T(8,128)S(1)}, u32[]{:S(2)}) copy-start(f32[16,1,128,128]{3,2,1,0:T(8,128)S(1)} %multiply_add_fusion) | copy-start | bytes 3145732
  109.1 9.7 %all-to-all-start.1 = ((f32[16,1,16]{2,1,0:T(1,128)}), f32[16,1,16]{2,1,0:T(1,128)S(1)}, u32[]{:S(2)}, u32[]{:S(2)}) async-start(f32[16,1,16]{2,1,0:T(1,128)} %broadcast_in_dim.2), calls=%async_computation.1 | async-start | bytes 16384 | tf_op jit(solution)/shard_map/all_to_all | solution.py:30
  233.5 13.4 %all-to-all-start.2 = ((f32[16,16,128]{2,1,0:T(8,128)}), f32[16,16,128]{2,1,0:T(8,128)S(1)}, u32[]{:S(2)}, u32[]{:S(2)}) async-start(f32[16,16,128]{2,1,0:T(8,128)} %bitcast.30), calls=%async_computation.2 | async-start | bytes 262144 | tf_op jit(solution)/shard_map/all_to_all | solution.py:24
Sparse Core Ops, SparseCore 0:
  10.7 77.1 all-gather.3
  90.1 68.8 all-gather.5
  161.1 68.5 all-gather.7
where the time goes:
time: 255 us; the launch traced here: 254 us
  blocking collectives  124 us (49%)
  waiting for transfers between devices  89.3 us (35%)
  between operations  13.9 us (5%)
  starting transfers between devices  10.1 us (4%)
  matrix products  9.56 us (4%)
  other arithmetic  4.07 us (2%)
  local copies, waits for them, and re-layouts  3.6 us (1%)
    all_gather x1, waiting for transfers between devices, shards(): lax.all_gather(w_down, 'tp', axis=1, tiled=True)  63.7 us
    all_gather x1, blocking collectives, shards(): lax.all_gather(w_mix_out, 'tp', axis=1, tiled=True)  44 us
    psum x1, blocking collectives, shards(): stream_total = lax.psum(jnp.sum(after_wide * after_wide, axis=1), 'kv')  30.4 us
    all_gather x1, blocking collectives, shards(): whole_rows = lax.all_gather(residual, 'kv', axis=1, tiled=True)  19.4 us
    all_gather x1, blocking collectives, shards(): hidden_in = lax.all_gather(hidden_own, 'kv', axis=1, tiled=True)  16.5 us
    all_gather x1, waiting for transfers between devices, side_by_side(): filled = lax.all_gather(both, axis, axis=dim, tiled=True)  13.5 us
    all_to_all x1, blocking collectives, summed_on_arrival(): lax.all_to_all(split_up(value, dim, devices), axis, 0, 0, tiled=True)  13.2 us
    all_to_all x1, starting transfers between devices, summed_on_arrival(): lax.all_to_all(split_up(value, dim, devices), axis, 0, 0, tiled=True)  6.53 us
  transfers between devices with their start and end apart: 5, of which 4 were waited for; matrix products, arithmetic and copies ran while one was open for 4% of the time, Pallas kernels for 0%

commit v1 on v0

--- a/solution.py
+++ b/solution.py
@@ -57,10 +57,23 @@
     w_up,
     w_down,
 ):
+
+    def mix_the_leaf(x_local):
+        dev_n = jax.lax.axis_size("kv")
+        sides = [(b, (b + 1) % dev_n) for b in range(dev_n)]
+        o_now = [None] * dev_n
+        o_now[dev_n - 1] = x_local
+        for m in range(dev_n - 2, -1, -1):
+            o_now[m] = jax.lax.ppermute(o_now[m + 1], axis_name="kv", perm=sides)
+        low = jnp.concatenate(o_now, 1)
+        prior = jax.lax.axis_index("kv")
+        right_arr = jnp.roll(low, (prior + 1) * x_local.shape[1], 1)
+        return right_arr
+
     batch_rows = residual.shape[0]
     own_cols = residual.shape[1]
     offset = lax.axis_index("kv") * own_cols
-    whole_rows = lax.all_gather(residual, "kv", axis=1, tiled=True)
+    whole_rows = mix_the_leaf(residual)
     full_width = whole_rows.shape[1]
     stream = whole_rows.astype(jnp.float32)
     normed = (stream * inverse_norm(stream) * gain_mix_pre).astype(jnp.bfloat16)

time: 255 us -> 289 us (1.13)
  the two profiles are of different devices: /device:TPU:1 before, /device:TPU:2 now
where the time goes in v1:
time: 289 us; the launch traced here: 287 us
  blocking collectives  107 us (37%)
  waiting for transfers between devices  106 us (37%)
  starting transfers between devices  40.4 us (14%)
  between operations  14.1 us (5%)
  matrix products  9.58 us (3%)
  local copies, waits for them, and re-layouts  5.24 us (2%)
  other arithmetic  4.06 us (1%)
    ppermute x15, waiting for transfers between devices, mix_the_leaf(): o_now[m] = jax.lax.ppermute(o_now[m + 1], axis_name='kv', perm=sides)  94.9 us
    psum x1, blocking collectives, shards(): stream_total = lax.psum(jnp.sum(after_wide * after_wide, axis=1), 'kv')  36.7 us
    all_gather x1, blocking collectives, shards(): lax.all_gather(w_mix_out, 'tp', axis=1, tiled=True)  33 us
    ppermute x15, starting transfers between devices, mix_the_leaf(): o_now[m] = jax.lax.ppermute(o_now[m + 1], axis_name='kv', perm=sides)  30.1 us
    all_gather x1, blocking collectives, shards(): hidden_in = lax.all_gather(hidden_own, 'kv', axis=1, tiled=True)  22.4 us
    all_to_all x1, blocking collectives, summed_on_arrival(): lax.all_to_all(split_up(value, dim, devices), axis, 0, 0, tiled=True)  15.1 us
    all_to_all x1, waiting for transfers between devices, summed_on_arrival(): lax.all_to_all(split_up(value, dim, devices), axis, 0, 0, tiled=True)  5.87 us
  transfers between devices with their start and end apart: 20, of which 16 were waited for; matrix products, arithmetic and copies ran while one was open for 4% of the time, Pallas kernels for 0%

profile of v1, /device:TPU:2, one launch (start us, length us, event | category | flops | bytes accessed | tf_op | source)
XLA Modules:
  0.0 286.8 jit_solution(17794049981838269960)
XLA Ops:
  9.6 3.4 %collective-permute-start = (bf16[16,128]{1,0:T(8,128)(2,1)}, bf16[16,128]{1,0:T(8,128)(2,1)S(1)}, u32[]{:S(2)}, u32[]{:S(2)}) collective-permute-start(bf16[16,128]{1,0:T(8,128)(2,1)} %param.15), channel_id=1, source_target_pairs={{0,32},{32,64},{64,96},{96,128},{128,160},{160,192},{192,224},{224... | collective-permute-start | bytes 12296 | tf_op jit(solution)/shard_map/ppermute | solution.py:67
  13.0 6.2 %collective-permute-done = bf16[16,128]{1,0:T(8,128)(2,1)S(1)} collective-permute-done((bf16[16,128]{1,0:T(8,128)(2,1)}, bf16[16,128]{1,0:T(8,128)(2,1)S(1)}, u32[]{:S(2)}, u32[]{:S(2)}) %collective-permute-start) | collective-permute-done | bytes 4128 | tf_op jit(solution)/shard_map/ppermute | solution.py:67
  19.1 1.9 collective-permute-start.1
  21.1 6.9 %collective-permute-done.1 = bf16[16,128]{1,0:T(8,128)(2,1)S(1)} collective-permute-done((bf16[16,128]{1,0:T(8,128)(2,1)S(1)}, bf16[16,128]{1,0:T(8,128)(2,1)S(1)}, u32[]{:S(2)}, u32[]{:S(2)}) %collective-permute-start.1) | collective-permute-done | bytes 4128 | tf_op jit(solution)/shard_map/ppermute | solution.py:67
  27.9 1.9 collective-permute-start.2
  29.9 6.9 %collective-permute-done.2 = bf16[16,128]{1,0:T(8,128)(2,1)S(1)} collective-permute-done((bf16[16,128]{1,0:T(8,128)(2,1)S(1)}, bf16[16,128]{1,0:T(8,128)(2,1)S(1)}, u32[]{:S(2)}, u32[]{:S(2)}) %collective-permute-start.2) | collective-permute-done | bytes 4128 | tf_op jit(solution)/shard_map/ppermute | solution.py:67
  36.8 1.9 collective-permute-start.3
  38.7 6.9 %collective-permute-done.3 = bf16[16,128]{1,0:T(8,128)(2,1)S(1)} collective-permute-done((bf16[16,128]{1,0:T(8,128)(2,1)S(1)}, bf16[16,128]{1,0:T(8,128)(2,1)S(1)}, u32[]{:S(2)}, u32[]{:S(2)}) %collective-permute-start.3) | collective-permute-done | bytes 4128 | tf_op jit(solution)/shard_map/ppermute | solution.py:67
  45.6 1.9 collective-permute-start.4
  47.5 6.9 %collective-permute-done.4 = bf16[16,128]{1,0:T(8,128)(2,1)S(1)} collective-permute-done((bf16[16,128]{1,0:T(8,128)(2,1)S(1)}, bf16[16,128]{1,0:T(8,128)(2,1)S(1)}, u32[]{:S(2)}, u32[]{:S(2)}) %collective-permute-start.4) | collective-permute-done | bytes 4128 | tf_op jit(solution)/shard_map/ppermute | solution.py:67
  54.4 1.9 collective-permute-start.5
  56.3 6.9 %collective-permute-done.5 = bf16[16,128]{1,0:T(8,128)(2,1)S(1)} collective-permute-done((bf16[16,128]{1,0:T(8,128)(2,1)S(1)}, bf16[16,128]{1,0:T(8,128)(2,1)S(1)}, u32[]{:S(2)}, u32[]{:S(2)}) %collective-permute-start.5) | collective-permute-done | bytes 4128 | tf_op jit(solution)/shard_map/ppermute | solution.py:67
  63.2 1.9 collective-permute-start.6
  65.1 6.9 %collective-permute-done.6 = bf16[16,128]{1,0:T(8,128)(2,1)S(1)} collective-permute-done((bf16[16,128]{1,0:T(8,128)(2,1)S(1)}, bf16[16,128]{1,0:T(8,128)(2,1)S(1)}, u32[]{:S(2)}, u32[]{:S(2)}) %collective-permute-start.6) | collective-permute-done | bytes 4128 | tf_op jit(solution)/shard_map/ppermute | solution.py:67
  72.0 1.9 collective-permute-start.7
  73.9 6.9 %collective-permute-done.7 = bf16[16,128]{1,0:T(8,128)(2,1)S(1)} collective-permute-done((bf16[16,128]{1,0:T(8,128)(2,1)S(1)}, bf16[16,128]{1,0:T(8,128)(2,1)S(1)}, u32[]{:S(2)}, u32[]{:S(2)}) %collective-permute-start.7) | collective-permute-done | bytes 4128 | tf_op jit(solution)/shard_map/ppermute | solution.py:67
  82.7 6.9 %collective-permute-done.8 = bf16[16,128]{1,0:T(8,128)(2,1)S(1)} collective-permute-done((bf16[16,128]{1,0:T(8,128)(2,1)S(1)}, bf16[16,128]{1,0:T(8,128)(2,1)S(1)}, u32[]{:S(2)}, u32[]{:S(2)}) %collective-permute-start.8) | collective-permute-done | bytes 4128 | tf_op jit(solution)/shard_map/ppermute | solution.py:67
  91.5 6.9 %collective-permute-done.9 = bf16[16,128]{1,0:T(8,128)(2,1)S(1)} collective-permute-done((bf16[16,128]{1,0:T(8,128)(2,1)S(1)}, bf16[16,128]{1,0:T(8,128)(2,1)S(1)}, u32[]{:S(2)}, u32[]{:S(2)}) %collective-permute-start.9) | collective-permute-done | bytes 4128 | tf_op jit(solution)/shard_map/ppermute | solution.py:67
  100.3 6.9 %collective-permute-done.10 = bf16[16,128]{1,0:T(8,128)(2,1)S(1)} collective-permute-done((bf16[16,128]{1,0:T(8,128)(2,1)S(1)}, bf16[16,128]{1,0:T(8,128)(2,1)S(1)}, u32[]{:S(2)}, u32[]{:S(2)}) %collective-permute-start.10) | collective-permute-done | bytes 4128 | tf_op jit(solution)/shard_map/ppermute | solution.py:67
  109.2 6.9 %collective-permute-done.11 = bf16[16,128]{1,0:T(8,128)(2,1)S(1)} collective-permute-done((bf16[16,128]{1,0:T(8,128)(2,1)S(1)}, bf16[16,128]{1,0:T(8,128)(2,1)S(1)}, u32[]{:S(2)}, u32[]{:S(2)}) %collective-permute-start.11) | collective-permute-done | bytes 4128 | tf_op jit(solution)/shard_map/ppermute | solution.py:67
  118.0 6.9 %collective-permute-done.12 = bf16[16,128]{1,0:T(8,128)(2,1)S(1)} collective-permute-done((bf16[16,128]{1,0:T(8,128)(2,1)S(1)}, bf16[16,128]{1,0:T(8,128)(2,1)S(1)}, u32[]{:S(2)}, u32[]{:S(2)}) %collective-permute-start.12) | collective-permute-done | bytes 4128 | tf_op jit(solution)/shard_map/ppermute | solution.py:67
  126.8 33.0 %all_gather.16 = bf16[128,2048]{0,1:T(8,128)(2,1)S(1)} all-gather(bf16[128,64]{0,1:T(8,128)(2,1)} %param.23), channel_id=1, replica_groups=mesh['kv'=16,'tp'=32] {'tp'}, dimensions={1}, use_global_device_ids=true | all-gather | bytes 540672 | tf_op jit(solution)/shard_map/all_gather | solution.py:110
  159.7 1.9 collective-permute-start.14
  162.3 6.0 %collective-permute-done.14 = bf16[16,128]{1,0:T(8,128)(2,1)S(1)} collective-permute-done((bf16[16,128]{1,0:T(8,128)(2,1)S(1)}, bf16[16,128]{1,0:T(8,128)(2,1)S(1)}, u32[]{:S(2)}, u32[]{:S(2)}) %collective-permute-start.14) | collective-permute-done | bytes 4128 | tf_op jit(solution)/shard_map/ppermute | solution.py:67
  177.4 15.1 %all_to_all.16 = f32[16,16,128]{2,1,0:T(8,128)S(1)} all-to-all(f32[16,16,128]{2,1,0:T(8,128)S(1)} %convolution_bitcast_fusion), channel_id=1, replica_groups=mesh['kv'=16,'tp'=32] {'kv'}, dimensions={0} | all-to-all | bytes 262144 | tf_op jit(solution)/shard_map/all_to_all | solution.py:24
  193.3 4.7 %all-to-all-start.1 = ((f32[16,1,16]{2,1,0:T(1,128)}), f32[16,1,16]{2,1,0:T(1,128)S(1)}, u32[]{:S(2)}, u32[]{:S(2)}) async-start(f32[16,1,16]{2,1,0:T(1,128)} %broadcast_in_dim.2), calls=%async_computation.1 | async-start | bytes 16384 | tf_op jit(solution)/shard_map/all_to_all | solution.py:30
  199.5 4.8 %all-to-all-done.1 = f32[16,1,16]{2,1,0:T(1,128)S(1)} async-done(((f32[16,1,16]{2,1,0:T(1,128)}), f32[16,1,16]{2,1,0:T(1,128)S(1)}, u32[]{:S(2)}, u32[]{:S(2)}) %all-to-all-start.1) | async-done | bytes 1056 | tf_op jit(solution)/shard_map/all_to_all | solution.py:30
  204.5 36.7 %psum.7 = f32[16]{0:T(128)S(1)} all-reduce(f32[16]{0:T(128)S(1)} %get-tuple-element.2), channel_id=1, replica_groups=mesh['kv'=16,'tp'=32] {'kv'}, use_global_device_ids=true, to_apply=%region_6.7 | all-reduce | flops 16 | bytes 128 | tf_op jit(solution)/shard_map/psum | solution.py:121
  241.3 22.4 %all_gather.17 = bf16[16,2048]{1,0:T(8,128)(2,1)S(1)} all-gather(bf16[16,128]{1,0:T(8,128)(2,1)S(1)} %fusion.32), channel_id=1, replica_groups=mesh['kv'=16,'tp'=32] {'kv'}, dimensions={1}, use_global_device_ids=true | all-gather | bytes 69632 | tf_op jit(solution)/shard_map/all_gather | solution.py:125
  263.7 3.2 %convolution_bitcast_fusion.1 = f32[2,16,8,128]{3,2,1,0:T(8,128)S(1)} fusion(bf16[512,2048]{0,1:T(8,128)(2,1)} %all-gather.8.cloned.1.call-done, bf16[16,2048]{1,0:T(8,128)(2,1)S(1)} %all_gather.17, bf16[2048,512]{1,0:T(8,128)(2,1)} %all-gather.6.cloned.1.call-done), kind=kOutput, calls=%fused_computation.1 | convolution fusion | flops 67133440 | bytes 4390912 | tf_op jit(solution)/shard_map/dot_general | solution.py:133
  267.6 5.4 %all-to-all-start.2 = ((f32[16,16,128]{2,1,0:T(8,128)}), f32[16,16,128]{2,1,0:T(8,128)S(1)}, u32[]{:S(2)}, u32[]{:S(2)}) async-start(f32[16,16,128]{2,1,0:T(8,128)} %bitcast.30), calls=%async_computation.2 | async-start | bytes 262144 | tf_op jit(solution)/shard_map/all_to_all | solution.py:24
  273.8 5.9 %all-to-all-done.2 = f32[16,16,128]{2,1,0:T(8,128)S(1)} async-done(((f32[16,16,128]{2,1,0:T(8,128)}), f32[16,16,128]{2,1,0:T(8,128)S(1)}, u32[]{:S(2)}, u32[]{:S(2)}) %all-to-all-start.2) | async-done | bytes 131104 | tf_op jit(solution)/shard_map/all_to_all | solution.py:24
  (86 shorter events, 28.0 us)
Async XLA Ops:
  7.2 165.7 %copy-start.5 = (f32[128]{0:T(128)S(1)}, f32[128]{0:T(128)}, u32[]{:S(2)}) copy-start(f32[128]{0:T(128)} %param.21) | copy-start | bytes 1540
  7.2 165.7 %copy-start.3 = (f32[2048]{0:T(1024)S(1)}, f32[2048]{0:T(1024)}, u32[]{:S(2)}) copy-start(f32[2048]{0:T(1024)} %param.24) | copy-start | bytes 24580
  7.2 167.0 %copy-start.1 = (f32[16,1,128,128]{3,2,1,0:T(8,128)S(1)}, f32[16,1,128,128]{3,2,1,0:T(8,128)}, u32[]{:S(2)}) copy-start(f32[16,1,128,128]{3,2,1,0:T(8,128)} %param.16) | copy-start | bytes 3145732
  7.2 163.0 %all-gather.4.cloned.1.call-start = ((), (), s32[]{:S(2)}) async-start(), calls=%async_computation.3 | async-start | bytes 2162688 | tf_op jit(solution)/shard_map/all_gather | solution.py:13
  8.8 255.0 %all-gather.6.cloned.1.call-start = ((), (), s32[]{:S(2)}) async-start(), calls=%async_computation.4 | async-start | bytes 2162688 | tf_op jit(solution)/shard_map/all_gather | solution.py:129
  9.5 254.2 %all-gather.8.cloned.1.call-start = ((), (), s32[]{:S(2)}) async-start(), calls=%async_computation.5 | async-start | bytes 2162688 | tf_op jit(solution)/shard_map/all_gather | solution.py:135
  9.6 9.6 %collective-permute-start = (bf16[16,128]{1,0:T(8,128)(2,1)}, bf16[16,128]{1,0:T(8,128)(2,1)S(1)}, u32[]{:S(2)}, u32[]{:S(2)}) collective-permute-start(bf16[16,128]{1,0:T(8,128)(2,1)} %param.15), channel_id=1, source_target_pairs={{0,32},{32,64},{64,96},{96,128},{128,160},{160,192},{192,224},{224... | collective-permute-start | bytes 12296 | tf_op jit(solution)/shard_map/ppermute | solution.py:67
  19.1 8.8 %collective-permute-start.1 = (bf16[16,128]{1,0:T(8,128)(2,1)S(1)}, bf16[16,128]{1,0:T(8,128)(2,1)S(1)}, u32[]{:S(2)}, u32[]{:S(2)}) collective-permute-start(bf16[16,128]{1,0:T(8,128)(2,1)S(1)} %collective-permute-done), channel_id=1, source_target_pairs={{0,32},{32,64},{64,96},{96,128},{128,160},{160,192},{192,224},{224... | collective-permute-start | bytes 12296 | tf_op jit(solution)/shard_map/ppermute | solution.py:67
  27.9 8.8 %collective-permute-start.2 = (bf16[16,128]{1,0:T(8,128)(2,1)S(1)}, bf16[16,128]{1,0:T(8,128)(2,1)S(1)}, u32[]{:S(2)}, u32[]{:S(2)}) collective-permute-start(bf16[16,128]{1,0:T(8,128)(2,1)S(1)} %collective-permute-done.1), channel_id=1, source_target_pairs={{0,32},{32,64},{64,96},{96,128},{128,160},{160,192},{192,224},{224... | collective-permute-start | bytes 12296 | tf_op jit(solution)/shard_map/ppermute | solution.py:67
  36.8 8.8 %collective-permute-start.3 = (bf16[16,128]{1,0:T(8,128)(2,1)S(1)}, bf16[16,128]{1,0:T(8,128)(2,1)S(1)}, u32[]{:S(2)}, u32[]{:S(2)}) collective-permute-start(bf16[16,128]{1,0:T(8,128)(2,1)S(1)} %collective-permute-done.2), channel_id=1, source_target_pairs={{0,32},{32,64},{64,96},{96,128},{128,160},{160,192},{192,224},{224... | collective-permute-start | bytes 12296 | tf_op jit(solution)/shard_map/ppermute | solution.py:67
  45.6 8.8 %collective-permute-start.4 = (bf16[16,128]{1,0:T(8,128)(2,1)S(1)}, bf16[16,128]{1,0:T(8,128)(2,1)S(1)}, u32[]{:S(2)}, u32[]{:S(2)}) collective-permute-start(bf16[16,128]{1,0:T(8,128)(2,1)S(1)} %collective-permute-done.3), channel_id=1, source_target_pairs={{0,32},{32,64},{64,96},{96,128},{128,160},{160,192},{192,224},{224... | collective-permute-start | bytes 12296 | tf_op jit(solution)/shard_map/ppermute | solution.py:67
  54.4 8.8 %collective-permute-start.5 = (bf16[16,128]{1,0:T(8,128)(2,1)S(1)}, bf16[16,128]{1,0:T(8,128)(2,1)S(1)}, u32[]{:S(2)}, u32[]{:S(2)}) collective-permute-start(bf16[16,128]{1,0:T(8,128)(2,1)S(1)} %collective-permute-done.4), channel_id=1, source_target_pairs={{0,32},{32,64},{64,96},{96,128},{128,160},{160,192},{192,224},{224... | collective-permute-start | bytes 12296 | tf_op jit(solution)/shard_map/ppermute | solution.py:67
  63.2 8.8 %collective-permute-start.6 = (bf16[16,128]{1,0:T(8,128)(2,1)S(1)}, bf16[16,128]{1,0:T(8,128)(2,1)S(1)}, u32[]{:S(2)}, u32[]{:S(2)}) collective-permute-start(bf16[16,128]{1,0:T(8,128)(2,1)S(1)} %collective-permute-done.5), channel_id=1, source_target_pairs={{0,32},{32,64},{64,96},{96,128},{128,160},{160,192},{192,224},{224... | collective-permute-start | bytes 12296 | tf_op jit(solution)/shard_map/ppermute | solution.py:67
  72.0 8.8 %collective-permute-start.7 = (bf16[16,128]{1,0:T(8,128)(2,1)S(1)}, bf16[16,128]{1,0:T(8,128)(2,1)S(1)}, u32[]{:S(2)}, u32[]{:S(2)}) collective-permute-start(bf16[16,128]{1,0:T(8,128)(2,1)S(1)} %collective-permute-done.6), channel_id=1, source_target_pairs={{0,32},{32,64},{64,96},{96,128},{128,160},{160,192},{192,224},{224... | collective-permute-start | bytes 12296 | tf_op jit(solution)/shard_map/ppermute | solution.py:67
  80.8 8.8 %collective-permute-start.8 = (bf16[16,128]{1,0:T(8,128)(2,1)S(1)}, bf16[16,128]{1,0:T(8,128)(2,1)S(1)}, u32[]{:S(2)}, u32[]{:S(2)}) collective-permute-start(bf16[16,128]{1,0:T(8,128)(2,1)S(1)} %collective-permute-done.7), channel_id=1, source_target_pairs={{0,32},{32,64},{64,96},{96,128},{128,160},{160,192},{192,224},{224... | collective-permute-start | bytes 12296 | tf_op jit(solution)/shard_map/ppermute | solution.py:67
  89.6 8.8 %collective-permute-start.9 = (bf16[16,128]{1,0:T(8,128)(2,1)S(1)}, bf16[16,128]{1,0:T(8,128)(2,1)S(1)}, u32[]{:S(2)}, u32[]{:S(2)}) collective-permute-start(bf16[16,128]{1,0:T(8,128)(2,1)S(1)} %collective-permute-done.8), channel_id=1, source_target_pairs={{0,32},{32,64},{64,96},{96,128},{128,160},{160,192},{192,224},{224... | collective-permute-start | bytes 12296 | tf_op jit(solution)/shard_map/ppermute | solution.py:67
  98.4 8.8 %collective-permute-start.10 = (bf16[16,128]{1,0:T(8,128)(2,1)S(1)}, bf16[16,128]{1,0:T(8,128)(2,1)S(1)}, u32[]{:S(2)}, u32[]{:S(2)}) collective-permute-start(bf16[16,128]{1,0:T(8,128)(2,1)S(1)} %collective-permute-done.9), channel_id=1, source_target_pairs={{0,32},{32,64},{64,96},{96,128},{128,160},{160,192},{192,224},{224... | collective-permute-start | bytes 12296 | tf_op jit(solution)/shard_map/ppermute | solution.py:67
  107.2 8.8 %collective-permute-start.11 = (bf16[16,128]{1,0:T(8,128)(2,1)S(1)}, bf16[16,128]{1,0:T(8,128)(2,1)S(1)}, u32[]{:S(2)}, u32[]{:S(2)}) collective-permute-start(bf16[16,128]{1,0:T(8,128)(2,1)S(1)} %collective-permute-done.10), channel_id=1, source_target_pairs={{0,32},{32,64},{64,96},{96,128},{128,160},{160,192},{192,224},{224... | collective-permute-start | bytes 12296 | tf_op jit(solution)/shard_map/ppermute | solution.py:67
  116.0 8.8 %collective-permute-start.12 = (bf16[16,128]{1,0:T(8,128)(2,1)S(1)}, bf16[16,128]{1,0:T(8,128)(2,1)S(1)}, u32[]{:S(2)}, u32[]{:S(2)}) collective-permute-start(bf16[16,128]{1,0:T(8,128)(2,1)S(1)} %collective-permute-done.11), channel_id=1, source_target_pairs={{0,32},{32,64},{64,96},{96,128},{128,160},{160,192},{192,224},{224... | collective-permute-start | bytes 12296 | tf_op jit(solution)/shard_map/ppermute | solution.py:67
  124.9 34.9 %collective-permute-start.13 = (bf16[16,128]{1,0:T(8,128)(2,1)S(1)}, bf16[16,128]{1,0:T(8,128)(2,1)S(1)}, u32[]{:S(2)}, u32[]{:S(2)}) collective-permute-start(bf16[16,128]{1,0:T(8,128)(2,1)S(1)} %collective-permute-done.12), channel_id=1, source_target_pairs={{0,32},{32,64},{64,96},{96,128},{128,160},{160,192},{192,224},{224... | collective-permute-start | bytes 12296 | tf_op jit(solution)/shard_map/ppermute | solution.py:67
  159.7 8.6 %collective-permute-start.14 = (bf16[16,128]{1,0:T(8,128)(2,1)S(1)}, bf16[16,128]{1,0:T(8,128)(2,1)S(1)}, u32[]{:S(2)}, u32[]{:S(2)}) collective-permute-start(bf16[16,128]{1,0:T(8,128)(2,1)S(1)} %collective-permute-done.13), channel_id=1, source_target_pairs={{0,32},{32,64},{64,96},{96,128},{128,160},{160,192},{192,224},{224... | collective-permute-start | bytes 12296 | tf_op jit(solution)/shard_map/ppermute | solution.py:67
  172.8 3.1 %copy-start.4 = (f32[128]{0:T(128)S(1)}, f32[128]{0:T(128)}, u32[]{:S(2)}) copy-start(f32[128]{0:T(128)} %param.22) | copy-start | bytes 1540
  174.2 30.2 %copy-start.2 = (bf16[16,128]{1,0:T(8,128)(2,1)S(1)}, bf16[16,128]{1,0:T(8,128)(2,1)}, u32[]{:S(2)}) copy-start(bf16[16,128]{1,0:T(8,128)(2,1)} %param.15) | copy-start | bytes 12292
  174.8 92.1 %copy-start = (f32[16,1,128,128]{3,2,1,0:T(8,128)}, f32[16,1,128,128]{3,2,1,0:T(8,128)S(1)}, u32[]{:S(2)}) copy-start(f32[16,1,128,128]{3,2,1,0:T(8,128)S(1)} %multiply_add_fusion) | copy-start | bytes 3145732
  193.3 11.0 %all-to-all-start.1 = ((f32[16,1,16]{2,1,0:T(1,128)}), f32[16,1,16]{2,1,0:T(1,128)S(1)}, u32[]{:S(2)}, u32[]{:S(2)}) async-start(f32[16,1,16]{2,1,0:T(1,128)} %broadcast_in_dim.2), calls=%async_computation.1 | async-start | bytes 16384 | tf_op jit(solution)/shard_map/all_to_all | solution.py:30
  267.6 12.0 %all-to-all-start.2 = ((f32[16,16,128]{2,1,0:T(8,128)}), f32[16,16,128]{2,1,0:T(8,128)S(1)}, u32[]{:S(2)}, u32[]{:S(2)}) async-start(f32[16,16,128]{2,1,0:T(8,128)} %bitcast.30), calls=%async_computation.2 | async-start | bytes 262144 | tf_op jit(solution)/shard_map/all_to_all | solution.py:24
Sparse Core Ops, SparseCore 0:
  10.7 75.8 all-gather.3
  88.7 68.6 all-gather.5
  159.6 68.3 all-gather.7
